TPU v7x, 32 devices: a whole 2x2x4 slice. The times are simulated.
32 devices in a mesh: sp: 4 (over y, x), tp: 8 (over z, core).
Axes of the slice: x: 2, y: 2, z: 4, core: 2. Of those that a mesh axis runs over, the one named last changes fastest.
Arguments:
- queries: bfloat16 [1536, 2048], P('sp', 'tp'), may hold values from -6 to 6
- keys: bfloat16 [1536, 2048], P('sp', 'tp'), may hold values from -6 to 6
- values: bfloat16 [1536, 2048], P('sp', 'tp'), may hold values from -6 to 6
- key_bias: bfloat16 [1536, 32], P('sp', 'tp'), may hold values from -16 to 0
- head_gain: float32 [32, 64], P('tp'), may hold values from 0.1 to 1.9
- out_weight: bfloat16 [2048, 2048], P('tp'), may hold values from -0.125 to 0.125
- residual: bfloat16 [1536, 2048], P(('sp', 'tp')), may hold values from -6 to 6
- norm_gain: float32 [2048], replicated, may hold values from 0.1 to 1.9
- gate_proj: bfloat16 [4, 2048, 7168], P('sp', None, 'tp'), may hold values from -0.125 to 0.125
- up_proj: bfloat16 [4, 2048, 7168], P('sp', None, 'tp'), may hold values from -0.125 to 0.125
- down_proj: bfloat16 [4, 7168, 2048], P('sp', 'tp'), may hold values from -0.0625 to 0.0625
- expert_choice: int32 [1536, 2], P(('sp', 'tp')), may hold values from 0 to 3, all different within a row; in each aligned block of 48 rows (0 to 47, 48 to 95, ...) at most 48 rows name the same one
- expert_weights: float32 [1536, 2], P(('sp', 'tp')), may hold values from 0.2 to 1
Outputs:
- layer_out: bfloat16 [1536, 2048], P(('sp', 'tp'))
Inputs may be any that keep to these rules, and one draw needn't show every extreme that they name: `expert_choice`: in each aligned block of 48 rows (the rows of one device), no expert is named more than 48 times; the two experts of a row differ.
All inputs are finite; a program needn't handle non-finite values.
Results may differ from a plain program's by a relative error of at most 0.019.
Values may be sent and summed in bfloat16 or wider, within the bound.
A program may use at most 128 MiB of HBM per device.

v0:
```python
import jax
import jax.numpy as jnp
from jax import lax
from jax.sharding import PartitionSpec as P

epsilon = 1e-06


def rms_scaled(values_in):
    return values_in * lax.rsqrt(jnp.mean(values_in * values_in, axis=-1, keepdims=True) + epsilon)


def expert_partial(row_block, gate_matrix, up_matrix, down_matrix):
    gate_part = jnp.dot(row_block, gate_matrix, preferred_element_type=jnp.float32)
    up_part = jnp.dot(row_block, up_matrix, preferred_element_type=jnp.float32)
    hidden = (jax.nn.silu(gate_part) * up_part).astype(jnp.bfloat16)
    return jnp.dot(hidden, down_matrix, preferred_element_type=jnp.float32)


def choice_ranks(routes, experts_all):
    flat_routes = routes.reshape(routes.shape[:-2] + (-1,))
    onehot = (flat_routes[..., None] == jnp.arange(experts_all, dtype=jnp.int32)).astype(jnp.int32)
    before = jnp.cumsum(onehot, axis=-2) - onehot
    return jnp.sum(before * onehot, axis=-1).reshape(routes.shape)


def slot_tokens(slot_index, targets, missing):
    flat_slots = slot_index.reshape(-1)
    owners = jnp.arange(flat_slots.shape[0], dtype=jnp.int32) // 2
    matches = flat_slots[None, :] == jnp.arange(targets, dtype=jnp.int32)[:, None]
    owner_found = jnp.sum(jnp.where(matches, owners[None, :], 0), axis=1)
    return jnp.where(jnp.any(matches, axis=1), owner_found, missing)


def on_device(
    queries,
    keys,
    values,
    key_bias,
    head_gain,
    out_weight,
    residual,
    norm_gain,
    gate_proj,
    up_proj,
    down_proj,
    expert_choice,
    expert_weights,
):
    rows_own = queries.shape[0]
    heads_here = head_gain.shape[0]
    head_size = head_gain.shape[1]
    model_width = out_weight.shape[1]
    seq_devices = lax.axis_size("sp")
    head_devices = lax.axis_size("tp")
    own_start = lax.axis_index("sp") * rows_own
    query_pos = own_start + jnp.arange(rows_own, dtype=jnp.int32)
    query_heads = queries.reshape(rows_own, heads_here, head_size)

    def key_block(slot_state, key_rows, value_rows, bias_rows, key_start):
        key_heads = key_rows.reshape(rows_own, heads_here, head_size)
        value_heads = value_rows.reshape(rows_own, heads_here, head_size)
        scores = jnp.einsum(
            "qhd,khd->hqk", query_heads, key_heads, preferred_element_type=jnp.float32
        ) * head_size ** (-0.5)
        scores = scores + bias_rows.astype(jnp.float32).T[:, None, :]
        key_pos = key_start + jnp.arange(rows_own, dtype=jnp.int32)
        earlier = (key_pos[None, :] < query_pos[:, None])[None, :, :]
        log_drops = jnp.where(earlier, jax.nn.log_sigmoid(-scores), 0.0)
        suffix = lax.cumsum(log_drops, axis=2, reverse=True) - log_drops
        within = jnp.where(earlier, jnp.exp(jax.nn.log_sigmoid(scores) + suffix), 0.0).astype(
            jnp.bfloat16
        )
        block_part = jnp.einsum(
            "hqk,khd->qhd", within, value_heads, preferred_element_type=jnp.float32
        )
        block_index = key_start // rows_own
        sums_new = lax.dynamic_update_index_in_dim(
            slot_state[0], block_part.reshape(rows_own, heads_here * head_size), block_index, 0
        )
        totals_new = lax.dynamic_update_index_in_dim(
            slot_state[1], jnp.sum(log_drops, axis=2), block_index, 0
        )
        return (sums_new, totals_new)

    empty_state = (
        jnp.zeros((seq_devices, rows_own, heads_here * head_size), jnp.float32),
        jnp.zeros((seq_devices, heads_here, rows_own), jnp.float32),
    )
    key_piece = lax.all_gather(keys, "sp", axis=0, tiled=True)
    value_piece = lax.all_gather(values, "sp", axis=0, tiled=True)
    bias_piece = lax.all_gather(key_bias, "sp", axis=0, tiled=True)

    def visit(block_count, state_in):
        offset = block_count * rows_own

        def take_rows(array):
            return lax.dynamic_slice_in_dim(array, offset, rows_own, 0)

        def compute(state_now):
            return key_block(
                state_now,
                take_rows(key_piece),
                take_rows(value_piece),
                take_rows(bias_piece),
                offset,
            )

        def keep(state_now):
            return state_now

        return lax.cond(offset <= own_start, compute, keep, state_in)

    block_sums, totals = lax.fori_loop(0, key_piece.shape[0] // rows_own, visit, empty_state)
    carried = jnp.sum(totals, axis=0, keepdims=True) - jnp.cumsum(totals, axis=0)
    factors = jnp.exp(carried).transpose(0, 2, 1)[..., None]
    mixture = jnp.sum(
        factors * block_sums.reshape(seq_devices, rows_own, heads_here, head_size), axis=0
    )
    attended = (
        (rms_scaled(mixture) * head_gain)
        .astype(jnp.bfloat16)
        .reshape(rows_own, heads_here * head_size)
    )
    row_share = rows_own // head_devices
    merged = lax.all_to_all(attended, "tp", split_axis=0, concat_axis=1, tiled=True)
    projected = jnp.dot(
        merged,
        lax.all_gather(out_weight, "tp", axis=0, tiled=True),
        preferred_element_type=jnp.float32,
    )
    stream = (residual.astype(jnp.float32) + projected).astype(jnp.bfloat16)
    normed = (rms_scaled(stream.astype(jnp.float32)) * norm_gain).astype(jnp.bfloat16)
    local_experts = gate_proj.shape[0]
    experts_all = local_experts * seq_devices
    capacity = 4 * rows_own // (head_devices * experts_all)
    own_slots = expert_choice * capacity + choice_ranks(expert_choice, experts_all)
    wanted = slot_tokens(own_slots, experts_all * capacity, row_share)
    outgoing = jnp.take(normed, wanted, axis=0, mode="fill", fill_value=0)
    arrived = lax.all_to_all(
        outgoing.reshape(seq_devices, local_experts, capacity, model_width),
        "sp",
        split_axis=0,
        concat_axis=0,
        tiled=True,
    )
    row_piece = lax.all_gather(arrived, "tp", axis=0, tiled=True)
    count_rows = row_piece.shape[0]
    partials = jnp.stack(
        [
            expert_partial(
                row_piece[:, 0].reshape(-1, model_width), gate_proj[0], up_proj[0], down_proj[0]
            ).reshape(count_rows, capacity, model_width)
        ],
        axis=1,
    )
    summed = lax.psum_scatter(partials.astype(jnp.bfloat16), "tp", scatter_dimension=0, tiled=True)
    returned = lax.all_to_all(summed, "sp", split_axis=0, concat_axis=0, tiled=True).reshape(
        experts_all * capacity, model_width
    )
    picked = jnp.take(returned, own_slots, axis=0).astype(jnp.float32)
    combined = jnp.sum(expert_weights[:, :, None] * picked, axis=1)
    return (stream.astype(jnp.float32) + combined).astype(jnp.bfloat16)


def solution(mesh):
    placed = (
        P("sp", "tp"),
        P("sp", "tp"),
        P("sp", "tp"),
        P("sp", "tp"),
        P("tp", None),
        P("tp", None),
        P(("sp", "tp"), None),
        P(),
        P("sp", None, "tp"),
        P("sp", None, "tp"),
        P("sp", "tp", None),
        P(("sp", "tp"), None),
        P(("sp", "tp"), None),
    )
    return jax.shard_map(
        on_device, mesh=mesh, in_specs=placed, out_specs=P(("sp", "tp"), None), check_vma=False
    )
```

profile of v0, /device:TPU:0, one launch (start us, length us, event | category | flops | bytes accessed | tf_op | source)
XLA Modules:
  0.0 380.5 jit_solution(13210839301603181166)
XLA Ops:
  9.4 1.7 copy.83
  11.2 11.0 %all_gather.17 = bf16[1536,4]{0,1:T(4,128)(2,1)} all-gather(bf16[384,4]{0,1:T(4,128)(2,1)} %param.20), channel_id=1, replica_groups=mesh['sp'=4,'tp'=8] {'sp'}, dimensions={0}, use_global_device_ids=true | all-gather | bytes 15360 | tf_op jit(solution)/shard_map/all_gather | solution.py:92
  22.2 12.4 %all_gather.15 = bf16[1536,256]{0,1:T(8,128)(2,1)} all-gather(bf16[384,256]{0,1:T(8,128)(2,1)S(1)} %copy.81), channel_id=1, replica_groups=mesh['sp'=4,'tp'=8] {'sp'}, dimensions={0}, use_global_device_ids=true | all-gather | bytes 983040 | tf_op jit(solution)/shard_map/all_gather | solution.py:91
  34.5 13.4 %all_gather.16 = bf16[1536,256]{0,1:T(8,128)(2,1)} all-gather(bf16[384,256]{0,1:T(8,128)(2,1)S(1)} %copy.82), channel_id=1, replica_groups=mesh['sp'=4,'tp'=8] {'sp'}, dimensions={0}, use_global_device_ids=true | all-gather | bytes 983040 | tf_op jit(solution)/shard_map/all_gather | solution.py:90
  47.9 1.3 broadcast_in_dim.84
  49.8 28.2 %while.17 = (s32[]{:T(128)}, f32[4,384,256]{1,2,0:T(8,128)}, f32[4,4,384]{2,1,0:T(4,128)}, s32[]{:T(128)}, bf16[1536,256]{0,1:T(8,128)(2,1)}, /*index=5*/bf16[15...) while((s32[]{:T(128)}, f32[4,384,256]{1,2,0:T(8,128)}, ...), condition=%wide.region_6.7_spmd.clone.clone, body=%wide.region_0.6_spmd.clone.clone.sunk | while | flops 246117120 | bytes 38572464 | solution.py:114
  49.8 28.0 %conditional.4 = ((f32[4,384,256]{1,2,0:T(8,128)}, f32[4,4,384]{2,1,0:T(4,128)})) conditional(s32[]{:T(128)} %convert_element_type.76, (f32[4,384,256]{1,2,0:T(8,128)}, f32[4,4,384]{2,1,0:T(4,128)}) %tuple.53, (s32[]{:T(128)}, bf16[1536,256]{0,1:T(8,128)(2,1)}, s32[]{:T(128)}, bf16[1536,256]{0,1:T(8,128)(2,1)}, bf16[384,4,64]{0,2,1:T(8,128)(2,1)}, ...), branch_computations={%region_1.0_spmd, %region_2.5_spmd} | conditional | flops 246117120 | bytes 38570716 | solution.py:112
  51.7 4.3 %fusion.15 = (f32[4,384]{1,0:T(4,128)S(1)}, f32[4,384,384]{1,2,0:T(8,128)S(1)}, f32[4,384,384]{2,1,0:T(8,128)}) fusion(f32[4,384]{1,0:T(4,128)S(1)} %convert_bitcast_fusion, pred[384,384]{0,1:T(8,128)(4,1)S(1)} %broadcast_compare_fusion, bf16[384,4,64]{0,2,1:T(8,128)(2,1)S(1)} %bitcast.92, bf16[384,4,64]{0,2,1:T(8,128)(2,1)} %get-tuple-element.177), kind=kOutput, calls=%fused_computation.33 | convolution fusion | flops 81984000 | bytes 5271552 | tf_op jit(solution)/shard_map/while/body/eval_jaxpr/cond/branch_1_fun/qhd,khd->hqk/dot_general | solution.py:63
  56.0 14.0 %fusion.2 = f32[4,384,3,128]{1,2,3,0:T(4,128)S(1)} fusion(f32[4,384,3,128]{1,3,2,0:T(8,128)S(1)} %bitcast.88), kind=kOutput, calls=%fused_computation.5 | output fusion | flops 74907648 | bytes 4718592 | tf_op jit(solution)/shard_map/reduce-window
  70.9 1.5 copy-done
  72.3 3.6 fusion.8
  79.5 1.6 fusion.22
  83.2 4.8 %all-to-all-start = ((bf16[8,48,256]{2,1,0:T(8,128)(2,1)}), bf16[8,48,256]{2,1,0:T(8,128)(2,1)S(1)}, u32[]{:S(2)}, u32[]{:S(2)}) async-start(bf16[8,48,256]{2,1,0:T(8,128)(2,1)} %multiply_convert_fusion.2), calls=%async_computation | async-start | bytes 393216 | tf_op jit(solution)/shard_map/all_to_all | solution.py:126
  89.5 6.8 %all-to-all-done = bf16[8,48,256]{2,1,0:T(8,128)(2,1)S(1)} async-done(((bf16[8,48,256]{2,1,0:T(8,128)(2,1)}), bf16[8,48,256]{2,1,0:T(8,128)(2,1)S(1)}, u32[]{:S(2)}, u32[]{:S(2)}) %all-to-all-start) | async-done | bytes 196640 | tf_op jit(solution)/shard_map/all_to_all | solution.py:126
  96.4 5.1 %multiply_reduce_fusion.1 = (f32[48]{0:T(128)S(1)}, f32[48,2048]{1,0:T(8,128)S(1)}) fusion(bf16[48,2048]{1,0:T(8,128)(2,1)S(1)} %bitcast.94, bf16[2048,2048]{1,0:T(8,128)(2,1)} %all-gather.3.cloned.1.call-done, bf16[48,2048]{1,0:T(8,128)(2,1)S(1)} %copy-done.1), kind=kOutput, calls=%fused_computation.54 | convolution fusion | flops 403242944 | bytes 9175232 | tf_op jit(solution)/shard_map/dot_general | solution.py:127
  102.9 96.4 %all_to_all.26 = bf16[4,1,48,2048]{3,2,1,0:T(8,128)(2,1)} all-to-all(bf16[4,1,48,2048]{3,2,1,0:T(8,128)(2,1)S(1)} %broadcast_select_fusion), channel_id=1, replica_groups=mesh['sp'=4,'tp'=8] {'sp'}, dimensions={0} | all-to-all | bytes 1572864 | tf_op jit(solution)/shard_map/all_to_all | solution.py:140
  199.4 63.5 %all-gather.5.cloned.1.call-done = bf16[32,1,48,2048]{3,2,1,0:T(8,128)(2,1)} async-done(((bf16[4,1,48,2048]{3,2,1,0:T(8,128)(2,1)}), bf16[32,1,48,2048]{3,2,1,0:T(8,128)(2,1)}) %all-gather.5.cloned.1.call-update) | async-done | bytes 6291472 | tf_op jit(solution)/shard_map/all_gather | solution.py:147
  262.9 10.0 %fusion.18 = f32[1536,896]{1,0:T(8,128)S(1)} fusion(bf16[1536,2048]{1,0:T(8,128)(2,1)} %bitcast.101, bf16[1,2048,896]{2,1,0:T(8,128)(2,1)} %param.25), kind=kOutput, calls=%fused_computation.38 | convolution fusion | flops 5637144576 | bytes 15466496 | tf_op jit(solution)/shard_map/dot_general | solution.py:14
  272.9 7.1 %multiply_convert_fusion = bf16[1536,896]{1,0:T(8,128)(2,1)S(1)} fusion(f32[1536,896]{1,0:T(8,128)S(1)} %fusion.18, bf16[1536,2048]{1,0:T(8,128)(2,1)S(1)} %bitcast.102, bf16[1,2048,896]{2,1,0:T(8,128)(2,1)S(1)} %copy-done.7), kind=kOutput, calls=%fused_computation.35 | convolution fusion | flops 5645402112 | bytes 18219008 | tf_op jit(solution)/shard_map/dot_general | solution.py:15
  280.0 8.7 %convert_bitcast_fusion.1 = bf16[32,1,48,2048]{3,2,0,1:T(8,128)(2,1)} fusion(bf16[32,48,896]{2,1,0:T(8,128)(2,1)S(1)} %bitcast.103, bf16[1,896,2048]{2,1,0:T(8,128)(2,1)S(1)} %copy-done.8), kind=kOutput, calls=%fused_computation.34 | convolution fusion | flops 5640290304 | bytes 12713984 | tf_op jit(solution)/shard_map/dot_general | solution.py:17
  288.8 68.5 %reduce-scatter.2.cloned.1.call-done = bf16[4,1,48,2048]{3,2,0,1:T(8,128)(2,1)} async-done(((bf16[32,1,48,2048]{3,2,0,1:T(8,128)(2,1)}), bf16[4,1,48,2048]{3,2,0,1:T(8,128)(2,1)}) %reduce-scatter.2.cloned.1.call-update) | async-done | bytes 786448 | tf_op jit(solution)/shard_map/reduce_scatter | solution.py:157
  357.3 3.7 all-to-all-start.2
  361.5 8.6 %all-to-all-done.2 = bf16[4,1,48,2048]{3,2,1,0:T(8,128)(2,1)S(1)} async-done(((bf16[4,1,48,2048]{3,2,1,0:T(8,128)(2,1)}), bf16[4,1,48,2048]{3,2,1,0:T(8,128)(2,1)S(1)}, u32[]{:S(2)}, u32[]{:S(2)}) %all-to-all-start.2) | async-done | bytes 786464 | tf_op jit(solution)/shard_map/all_to_all | solution.py:158
  371.2 2.1 multiply_reduce_fusion
  (88 shorter events, 16.8 us)
Async XLA Ops:
  6.5 89.9 %all-gather.3.cloned.1.call-start = ((), (), s32[]{:S(2)}) async-start(), calls=%async_computation.4 | async-start | bytes 9437184 | tf_op jit(solution)/shard_map/all_gather | solution.py:129
  70.6 1.7 copy-start
  79.5 2.9 copy-start.4
  81.1 7.0 %copy-start.3 = (s32[48,2]{0,1:T(2,128)S(1)}, s32[48,2]{0,1:T(2,128)}, u32[]{:S(2)}) copy-start(s32[48,2]{0,1:T(2,128)} %param.28) | copy-start | bytes 1156
  81.3 15.1 %copy-start.1 = (bf16[48,2048]{1,0:T(8,128)(2,1)S(1)}, bf16[48,2048]{1,0:T(8,128)(2,1)}, u32[]{:S(2)}) copy-start(bf16[48,2048]{1,0:T(8,128)(2,1)} %param.23) | copy-start | bytes 589828
  83.2 13.1 %all-to-all-start = ((bf16[8,48,256]{2,1,0:T(8,128)(2,1)}), bf16[8,48,256]{2,1,0:T(8,128)(2,1)S(1)}, u32[]{:S(2)}, u32[]{:S(2)}) async-start(bf16[8,48,256]{2,1,0:T(8,128)(2,1)} %multiply_convert_fusion.2), calls=%async_computation | async-start | bytes 393216 | tf_op jit(solution)/shard_map/all_to_all | solution.py:126
  88.0 174.9 %all-gather.5.cloned.1.call-start = ((), (), s32[]{:S(2)}) async-start(), calls=%async_computation.5 | async-start | bytes 7077888 | tf_op jit(solution)/shard_map/all_gather | solution.py:147
  96.4 5.1 %copy-start.2 = (f32[2048]{0:T(1024)S(1)}, f32[2048]{0:T(1024)}, u32[]{:S(2)}) copy-start(f32[2048]{0:T(1024)} %param.24) | copy-start | bytes 24580
  199.3 158.0 %reduce-scatter.2.cloned.1.call-start = ((), (), s32[]{:S(2)}) async-start(), calls=%async_computation.6 | async-start | bytes 7077888 | tf_op jit(solution)/shard_map/reduce_scatter | solution.py:157
  262.9 10.0 %copy-start.6 = (bf16[32,1,48,2048]{3,2,1,0:T(8,128)(2,1)S(1)}, bf16[32,1,48,2048]{3,2,1,0:T(8,128)(2,1)}, u32[]{:S(2)}) copy-start(bf16[32,1,48,2048]{3,2,1,0:T(8,128)(2,1)} %all-gather.5.cloned.1.call-done) | copy-start | bytes 18874372
  262.9 10.0 %copy-start.7 = (bf16[1,2048,896]{2,1,0:T(8,128)(2,1)S(1)}, bf16[1,2048,896]{2,1,0:T(8,128)(2,1)}, u32[]{:S(2)}) copy-start(bf16[1,2048,896]{2,1,0:T(8,128)(2,1)} %param.26) | copy-start | bytes 11010052
  272.9 7.1 %copy-start.8 = (bf16[1,896,2048]{2,1,0:T(8,128)(2,1)S(1)}, bf16[1,896,2048]{2,1,0:T(8,128)(2,1)}, u32[]{:S(2)}) copy-start(bf16[1,896,2048]{2,1,0:T(8,128)(2,1)} %param.27) | copy-start | bytes 11010052
  288.8 72.6 %copy-start.5 = (f32[48,2]{0,1:T(2,128)S(1)}, f32[48,2]{0,1:T(2,128)}, u32[]{:S(2)}) copy-start(f32[48,2]{0,1:T(2,128)} %param.29) | copy-start | bytes 1156
  357.3 12.7 %all-to-all-start.2 = ((bf16[4,1,48,2048]{3,2,1,0:T(8,128)(2,1)}), bf16[4,1,48,2048]{3,2,1,0:T(8,128)(2,1)S(1)}, u32[]{:S(2)}, u32[]{:S(2)}) async-start(bf16[4,1,48,2048]{3,2,1,0:T(8,128)(2,1)} %bitcast.96), calls=%async_computation.3 | async-start | bytes 1572864 | tf_op jit(solution)/shard_map/all_to_all | solution.py:158
Sparse Core Ops, SparseCore 0:
  8.9 84.8 all-gather.2
  199.4 63.4 all-gather.4
  288.9 68.3 reduce-scatter.1
where the time goes:
time: 382 us; the launch traced here: 380 us
  waiting for transfers between devices  148 us (39%)
  blocking collectives  133 us (35%)
  matrix products  35.5 us (9%)
  other arithmetic  26.7 us (7%)
  local copies, waits for them, and re-layouts  14.7 us (4%)
  between operations  13.4 us (4%)
  starting transfers between devices  8.62 us (2%)
    all_to_all x1, blocking collectives, on_device(): lax.all_to_all(outgoing.reshape(seq_devices, local_experts, capacity, mod...  96.4 us
    reduce_scatter x1, waiting for transfers between devices, on_device(): lax.psum_scatter(partials.astype(jnp.bfloat16), 'tp', scatter_dimension=0...  68.5 us
    all_gather x1, waiting for transfers between devices, on_device(): row_piece = lax.all_gather(arrived, 'tp', axis=0, tiled=True)  63.5 us
    another operation x2, other arithmetic  14.1 us
    all_gather x1, blocking collectives, on_device(): key_piece = lax.all_gather(keys, 'sp', axis=0, tiled=True)  13.4 us
    all_gather x1, blocking collectives, on_device(): value_piece = lax.all_gather(values, 'sp', axis=0, tiled=True)  12.4 us
    all_gather x1, blocking collectives, on_device(): bias_piece = lax.all_gather(key_bias, 'sp', axis=0, tiled=True)  11 us
    dot_general x1, matrix products, expert_partial(): jnp.dot(row_block, gate_matrix, preferred_element_type=jnp.float32)  9.96 us
  transfers between devices with their start and end apart: 5, of which 4 were waited for; matrix products, arithmetic and copies ran while one was open for 10% of the time, Pallas kernels for 0%

commit v1 on v0

--- a/solution.py
+++ b/solution.py
@@ -4,6 +4,27 @@
 from jax.sharding import PartitionSpec as P
 
 epsilon = 1e-06
+
+
+def _name_rings(v0, mesh_ax):
+    prior, w1, vec_out = (lax.axis_size(mesh_ax), lax.axis_index(mesh_ax), v0.shape[0])
+    bank = [(c, (c + 1) % prior) for c in range(prior)]
+    table = [(c, (c - 1) % prior) for c in range(prior)]
+    carry = jnp.zeros((*v0.shape[:0], prior * vec_out, *v0.shape[1:]), v0.dtype)
+    carry = lax.dynamic_update_slice_in_dim(carry, v0, w1 * vec_out, axis=0)
+    part_now = current_block = v0
+    u1 = prior // 2
+    for to_i in [*range(1, u1 + 1)]:
+        part_now = lax.ppermute(part_now, axis_name=mesh_ax, perm=bank)
+        carry = lax.dynamic_update_slice_in_dim(
+            carry, part_now, (w1 - to_i) % prior * vec_out, axis=0
+        )
+        if to_i < prior - u1:
+            current_block = lax.ppermute(current_block, axis_name=mesh_ax, perm=table)
+            carry = lax.dynamic_update_slice_in_dim(
+                carry, current_block, (w1 + to_i) % prior * vec_out, axis=0
+            )
+    return carry
 
 
 def rms_scaled(values_in):
@@ -144,7 +165,7 @@
         concat_axis=0,
         tiled=True,
     )
-    row_piece = lax.all_gather(arrived, "tp", axis=0, tiled=True)
+    row_piece = _name_rings(arrived, "tp")
     count_rows = row_piece.shape[0]
     partials = jnp.stack(
         [

time: 382 us -> 396 us (1.037)
  starting transfers between devices: 8.62 us -> 19.1 us
  loops' own time: 0.31 us -> 8.2 us
  waiting for transfers between devices: 148 us -> 144 us
    all_gather x1 -> x0, waiting for transfers between devices: 63.5 us -> none  [on_device(): row_piece = lax.all_gather(arrived, 'tp', axis=0, tiled=True)]
    ppermute x0 -> x7, waiting for transfers between devices: none -> 61.7 us  [the longest x4 60.1 us: _name_rings(): part_now = lax.ppermute(part_now, axis_name=mesh_ax, perm=bank)]
    ppermute x0 -> x7, starting transfers between devices: none -> 10.7 us  [the longest x3 10.7 us: _name_rings(): current_block = lax.ppermute(current_block, axis_name=mesh_ax, perm=table)]
    another operation x1, loops' own time: 0.2 us -> 8.08 us  [on_device(): lax.fori_loop(0, key_piece.shape[0] // rows_own, visit, empty_state)]
  transfers between devices with their start and end apart: 5 -> 11, of which waited for: 4 -> 8; matrix products, arithmetic and copies ran while one was open for 10% -> 11% of each run, Pallas kernels for 0% -> 0%
where the time goes in v1:
time: 396 us; the launch traced here: 395 us
  waiting for transfers between devices  144 us (36%)
  blocking collectives  133 us (34%)
  matrix products  32.4 us (8%)
  other arithmetic  26.7 us (7%)
  starting transfers between devices  19.1 us (5%)
  local copies, waits for them, and re-layouts  17.5 us (4%)
  between operations  14.1 us (4%)
  loops' own time  8.2 us (2%)
    all_to_all x1, blocking collectives, on_device(): lax.all_to_all(outgoing.reshape(seq_devices, local_experts, capacity, mod...  96.2 us
    reduce_scatter x1, waiting for transfers between devices, on_device(): lax.psum_scatter(partials.astype(jnp.bfloat16), 'tp', scatter_dimension=0...  66.6 us
    ppermute x4, waiting for transfers between devices, _name_rings(): part_now = lax.ppermute(part_now, axis_name=mesh_ax, perm=bank)  60.1 us
    another operation x2, other arithmetic  14.1 us
    all_gather x1, blocking collectives, on_device(): key_piece = lax.all_gather(keys, 'sp', axis=0, tiled=True)  13.4 us
    all_gather x1, blocking collectives, on_device(): value_piece = lax.all_gather(values, 'sp', axis=0, tiled=True)  12.4 us
    all_gather x1, blocking collectives, on_device(): bias_piece = lax.all_gather(key_bias, 'sp', axis=0, tiled=True)  11 us
    ppermute x3, starting transfers between devices, _name_rings(): current_block = lax.ppermute(current_block, axis_name=mesh_ax, perm=table)  10.7 us
  transfers between devices with their start and end apart: 11, of which 8 were waited for; matrix products, arithmetic and copies ran while one was open for 11% of the time, Pallas kernels for 0%

profile of v1, /device:TPU:0, one launch (start us, length us, event | category | flops | bytes accessed | tf_op | source)
XLA Modules:
  0.0 395.4 jit_solution(16256945131953297244)
XLA Ops:
  11.2 11.0 %all_gather.14 = bf16[1536,4]{0,1:T(4,128)(2,1)} all-gather(bf16[384,4]{0,1:T(4,128)(2,1)} %param.20), channel_id=1, replica_groups=mesh['sp'=4,'tp'=8] {'sp'}, dimensions={0}, use_global_device_ids=true | all-gather | bytes 15360 | tf_op jit(solution)/shard_map/all_gather | solution.py:113
  22.2 12.4 %all_gather.12 = bf16[1536,256]{0,1:T(8,128)(2,1)} all-gather(bf16[384,256]{0,1:T(8,128)(2,1)S(1)} %copy.81), channel_id=1, replica_groups=mesh['sp'=4,'tp'=8] {'sp'}, dimensions={0}, use_global_device_ids=true | all-gather | bytes 983040 | tf_op jit(solution)/shard_map/all_gather | solution.py:112
  34.5 13.4 %all_gather.13 = bf16[1536,256]{0,1:T(8,128)(2,1)} all-gather(bf16[384,256]{0,1:T(8,128)(2,1)S(1)} %copy.82), channel_id=1, replica_groups=mesh['sp'=4,'tp'=8] {'sp'}, dimensions={0}, use_global_device_ids=true | all-gather | bytes 983040 | tf_op jit(solution)/shard_map/all_gather | solution.py:111
  49.8 36.1 %while.17 = (s32[]{:T(128)}, f32[4,384,256]{1,2,0:T(8,128)}, f32[4,4,384]{2,1,0:T(4,128)}, s32[]{:T(128)}, bf16[1536,256]{0,1:T(8,128)(2,1)}, /*index=5*/bf16[15...) while((s32[]{:T(128)}, f32[4,384,256]{1,2,0:T(8,128)}, ...), condition=%wide.region_6.7_spmd.clone.clone, body=%wide.region_0.6_spmd.clone.clone.sunk | while | flops 246117120 | bytes 38572464 | solution.py:135
  49.8 28.0 %conditional.4 = ((f32[4,384,256]{1,2,0:T(8,128)}, f32[4,4,384]{2,1,0:T(4,128)})) conditional(s32[]{:T(128)} %convert_element_type.76, (f32[4,384,256]{1,2,0:T(8,128)}, f32[4,4,384]{2,1,0:T(4,128)}) %tuple.53, (s32[]{:T(128)}, bf16[1536,256]{0,1:T(8,128)(2,1)}, s32[]{:T(128)}, bf16[1536,256]{0,1:T(8,128)(2,1)}, bf16[384,4,64]{0,2,1:T(8,128)(2,1)}, ...), branch_computations={%region_1.0_spmd, %region_2.5_spmd} | conditional | flops 246117120 | bytes 38570716 | solution.py:133
  51.7 4.3 %fusion.15 = (f32[4,384]{1,0:T(4,128)S(1)}, f32[4,384,384]{1,2,0:T(8,128)S(1)}, f32[4,384,384]{2,1,0:T(8,128)}) fusion(f32[4,384]{1,0:T(4,128)S(1)} %convert_bitcast_fusion, pred[384,384]{0,1:T(8,128)(4,1)S(1)} %broadcast_compare_fusion, bf16[384,4,64]{0,2,1:T(8,128)(2,1)S(1)} %bitcast.96, bf16[384,4,64]{0,2,1:T(8,128)(2,1)} %get-tuple-element.177), kind=kOutput, calls=%fused_computation.33 | convolution fusion | flops 81984000 | bytes 5271552 | tf_op jit(solution)/shard_map/while/body/eval_jaxpr/cond/branch_1_fun/qhd,khd->hqk/dot_general | solution.py:84
  56.0 14.0 %fusion.2 = f32[4,384,3,128]{1,2,3,0:T(4,128)S(1)} fusion(f32[4,384,3,128]{1,3,2,0:T(8,128)S(1)} %bitcast.90), kind=kOutput, calls=%fused_computation.5 | output fusion | flops 74907648 | bytes 4718592 | tf_op jit(solution)/shard_map/reduce-window
  72.3 3.6 fusion.8
  91.1 4.8 %all-to-all-start = ((bf16[8,48,256]{2,1,0:T(8,128)(2,1)}), bf16[8,48,256]{2,1,0:T(8,128)(2,1)S(1)}, u32[]{:S(2)}, u32[]{:S(2)}) async-start(bf16[8,48,256]{2,1,0:T(8,128)(2,1)} %multiply_convert_fusion.2), calls=%async_computation | async-start | bytes 393216 | tf_op jit(solution)/shard_map/all_to_all | solution.py:147
  97.4 6.8 %all-to-all-done = bf16[8,48,256]{2,1,0:T(8,128)(2,1)S(1)} async-done(((bf16[8,48,256]{2,1,0:T(8,128)(2,1)}), bf16[8,48,256]{2,1,0:T(8,128)(2,1)S(1)}, u32[]{:S(2)}, u32[]{:S(2)}) %all-to-all-start) | async-done | bytes 196640 | tf_op jit(solution)/shard_map/all_to_all | solution.py:147
  104.3 5.1 %multiply_reduce_fusion.1 = (f32[48]{0:T(128)S(1)}, f32[48,2048]{1,0:T(8,128)S(1)}) fusion(bf16[48,2048]{1,0:T(8,128)(2,1)S(1)} %bitcast.98, bf16[2048,2048]{1,0:T(8,128)(2,1)} %all-gather.2.cloned.1.call-done, bf16[48,2048]{1,0:T(8,128)(2,1)S(1)} %copy-done.3), kind=kOutput, calls=%fused_computation.55 | convolution fusion | flops 403242944 | bytes 9175232 | tf_op jit(solution)/shard_map/dot_general | solution.py:148
  110.8 96.2 %all_to_all.26 = bf16[4,1,48,2048]{3,2,1,0:T(8,128)(2,1)S(1)} all-to-all(bf16[4,1,48,2048]{3,2,1,0:T(8,128)(2,1)S(1)} %broadcast_select_fusion), channel_id=1, replica_groups=mesh['sp'=4,'tp'=8] {'sp'}, dimensions={0} | all-to-all | bytes 1572864 | tf_op jit(solution)/shard_map/all_to_all | solution.py:161
  207.0 3.5 collective-permute-start.1
  210.5 17.1 %collective-permute-done = bf16[4,1,48,2048]{3,2,1,0:T(8,128)(2,1)S(1)} collective-permute-done((bf16[4,1,48,2048]{3,2,1,0:T(8,128)(2,1)S(1)}, bf16[4,1,48,2048]{3,2,1,0:T(8,128)(2,1)S(1)}, u32[]{:S(2)}, u32[]{:S(2)}) %collective-permute-start) | collective-permute-done | bytes 786464 | tf_op jit(solution)/shard_map/ppermute | solution.py:18
  231.2 17.9 %collective-permute-done.2 = bf16[4,1,48,2048]{3,2,1,0:T(8,128)(2,1)S(1)} collective-permute-done((bf16[4,1,48,2048]{3,2,1,0:T(8,128)(2,1)S(1)}, bf16[4,1,48,2048]{3,2,1,0:T(8,128)(2,1)S(1)}, u32[]{:S(2)}, u32[]{:S(2)}) %collective-permute-start.2) | collective-permute-done | bytes 786464 | tf_op jit(solution)/shard_map/ppermute | solution.py:18
  250.3 3.6 collective-permute-start.5
  255.1 13.9 %collective-permute-done.4 = bf16[4,1,48,2048]{3,2,1,0:T(8,128)(2,1)S(1)} collective-permute-done((bf16[4,1,48,2048]{3,2,1,0:T(8,128)(2,1)S(1)}, bf16[4,1,48,2048]{3,2,1,0:T(8,128)(2,1)S(1)}, u32[]{:S(2)}, u32[]{:S(2)}) %collective-permute-start.4) | collective-permute-done | bytes 786464 | tf_op jit(solution)/shard_map/ppermute | solution.py:18
  270.9 11.2 %collective-permute-done.6 = bf16[4,1,48,2048]{3,2,1,0:T(8,128)(2,1)S(1)} collective-permute-done((bf16[4,1,48,2048]{3,2,1,0:T(8,128)(2,1)S(1)}, bf16[4,1,48,2048]{3,2,1,0:T(8,128)(2,1)S(1)}, u32[]{:S(2)}, u32[]{:S(2)}) %collective-permute-start.6) | collective-permute-done | bytes 786464 | tf_op jit(solution)/shard_map/ppermute | solution.py:18
  282.3 6.7 %fusion.21 = f32[1536,896]{1,0:T(8,128)S(1)} fusion(bf16[1536,2048]{1,0:T(8,128)(2,1)S(1)} %bitcast.94, bf16[1,2048,896]{2,1,0:T(8,128)(2,1)S(1)} %copy-done.8), kind=kOutput, calls=%fused_computation.39 | convolution fusion | flops 5637144576 | bytes 15466496 | tf_op jit(solution)/shard_map/dot_general | solution.py:35
  289.0 7.3 %multiply_convert_fusion = bf16[1536,896]{1,0:T(8,128)(2,1)S(1)} fusion(f32[1536,896]{1,0:T(8,128)S(1)} %fusion.21, bf16[1536,2048]{1,0:T(8,128)(2,1)S(1)} %bitcast.95, bf16[1,2048,896]{2,1,0:T(8,128)(2,1)S(1)} %copy-done.9), kind=kOutput, calls=%fused_computation.35 | convolution fusion | flops 5645402112 | bytes 18219008 | tf_op jit(solution)/shard_map/dot_general | solution.py:36
  296.3 8.7 %convert_bitcast_fusion.1 = bf16[32,1,48,2048]{3,2,0,1:T(8,128)(2,1)} fusion(bf16[32,48,896]{2,1,0:T(8,128)(2,1)S(1)} %bitcast.105, bf16[1,896,2048]{2,1,0:T(8,128)(2,1)S(1)} %copy-done.10), kind=kOutput, calls=%fused_computation.34 | convolution fusion | flops 5640290304 | bytes 12713984 | tf_op jit(solution)/shard_map/dot_general | solution.py:38
  305.1 66.6 %reduce-scatter.2.cloned.1.call-done = bf16[4,1,48,2048]{3,2,0,1:T(8,128)(2,1)} async-done(((bf16[32,1,48,2048]{3,2,0,1:T(8,128)(2,1)}), bf16[4,1,48,2048]{3,2,0,1:T(8,128)(2,1)}) %reduce-scatter.2.cloned.1.call-update) | async-done | bytes 786448 | tf_op jit(solution)/shard_map/reduce_scatter | solution.py:178
  371.6 3.6 all-to-all-start.2
  375.7 8.7 %all-to-all-done.2 = bf16[4,1,48,2048]{3,2,1,0:T(8,128)(2,1)S(1)} async-done(((bf16[4,1,48,2048]{3,2,1,0:T(8,128)(2,1)}), bf16[4,1,48,2048]{3,2,1,0:T(8,128)(2,1)S(1)}, u32[]{:S(2)}, u32[]{:S(2)}) %all-to-all-start.2) | async-done | bytes 786464 | tf_op jit(solution)/shard_map/all_to_all | solution.py:179
  (112 shorter events, 32.8 us)
Async XLA Ops:
  6.5 97.7 %all-gather.2.cloned.1.call-start = ((), (), s32[]{:S(2)}) async-start(), calls=%async_computation.4 | async-start | bytes 9437184 | tf_op jit(solution)/shard_map/all_gather | solution.py:150
  70.6 1.7 copy-start
  85.8 4.5 %copy-start.6 = (f32[4,64]{1,0:T(4,128)S(1)}, f32[4,64]{1,0:T(4,128)}, u32[]{:S(2)}) copy-start(f32[4,64]{1,0:T(4,128)} %param.21) | copy-start | bytes 3076
  87.4 8.6 %copy-start.5 = (s32[48,2]{0,1:T(2,128)S(1)}, s32[48,2]{0,1:T(2,128)}, u32[]{:S(2)}) copy-start(s32[48,2]{0,1:T(2,128)} %param.28) | copy-start | bytes 1156
  89.0 15.3 %copy-start.3 = (bf16[48,2048]{1,0:T(8,128)(2,1)S(1)}, bf16[48,2048]{1,0:T(8,128)(2,1)}, u32[]{:S(2)}) copy-start(bf16[48,2048]{1,0:T(8,128)(2,1)} %param.23) | copy-start | bytes 589828
  91.1 13.1 %all-to-all-start = ((bf16[8,48,256]{2,1,0:T(8,128)(2,1)}), bf16[8,48,256]{2,1,0:T(8,128)(2,1)S(1)}, u32[]{:S(2)}, u32[]{:S(2)}) async-start(bf16[8,48,256]{2,1,0:T(8,128)(2,1)} %multiply_convert_fusion.2), calls=%async_computation | async-start | bytes 393216 | tf_op jit(solution)/shard_map/all_to_all | solution.py:147
  95.9 275.7 %reduce-scatter.2.cloned.1.call-start = ((), (), s32[]{:S(2)}) async-start(), calls=%async_computation.5 | async-start | bytes 7077888 | tf_op jit(solution)/shard_map/reduce_scatter | solution.py:178
  104.3 5.1 %copy-start.4 = (f32[2048]{0:T(1024)S(1)}, f32[2048]{0:T(1024)}, u32[]{:S(2)}) copy-start(f32[2048]{0:T(1024)} %param.24) | copy-start | bytes 24580
  207.0 20.6 %collective-permute-start = (bf16[4,1,48,2048]{3,2,1,0:T(8,128)(2,1)S(1)}, bf16[4,1,48,2048]{3,2,1,0:T(8,128)(2,1)S(1)}, u32[]{:S(2)}, u32[]{:S(2)}) collective-permute-start(bf16[4,1,48,2048]{3,2,1,0:T(8,128)(2,1)S(1)} %all_to_all.26), channel_id=1, source_target_pairs={{0,1},{1,2},{2,3},{3,4},{4,5},{5,6},{6,7},{7,0},{8,9},{9,10},{10,1... | collective-permute-start | bytes 2359304 | tf_op jit(solution)/shard_map/ppermute | solution.py:18
  207.0 20.6 %collective-permute-start.1 = (bf16[4,1,48,2048]{3,2,1,0:T(8,128)(2,1)S(1)}, bf16[4,1,48,2048]{3,2,1,0:T(8,128)(2,1)}, u32[]{:S(2)}, u32[]{:S(2)}) collective-permute-start(bf16[4,1,48,2048]{3,2,1,0:T(8,128)(2,1)S(1)} %all_to_all.26), channel_id=1, source_target_pairs={{0,7},{1,0},{2,1},{3,2},{4,3},{5,4},{6,5},{7,6},{8,15},{9,8},{10,9... | collective-permute-start | bytes 2359304 | tf_op jit(solution)/shard_map/ppermute | solution.py:23
  227.6 3.6 copy-start.1
  227.6 21.4 %collective-permute-start.2 = (bf16[4,1,48,2048]{3,2,1,0:T(8,128)(2,1)S(1)}, bf16[4,1,48,2048]{3,2,1,0:T(8,128)(2,1)S(1)}, u32[]{:S(2)}, u32[]{:S(2)}) collective-permute-start(bf16[4,1,48,2048]{3,2,1,0:T(8,128)(2,1)S(1)} %collective-permute-done), channel_id=1, source_target_pairs={{0,1},{1,2},{2,3},{3,4},{4,5},{5,6},{6,7},{7,0},{8,9},{9,10},{10,1... | collective-permute-start | bytes 2359304 | tf_op jit(solution)/shard_map/ppermute | solution.py:18
  227.6 22.6 %collective-permute-start.3 = (bf16[4,1,48,2048]{3,2,1,0:T(8,128)(2,1)}, bf16[4,1,48,2048]{3,2,1,0:T(8,128)(2,1)S(1)}, u32[]{:S(2)}, u32[]{:S(2)}) collective-permute-start(bf16[4,1,48,2048]{3,2,1,0:T(8,128)(2,1)} %collective-permute-done.1), channel_id=1, source_target_pairs={{0,7},{1,0},{2,1},{3,2},{4,3},{5,4},{6,5},{7,6},{8,15},{9,8},{10,9... | collective-permute-start | bytes 2359304 | tf_op jit(solution)/shard_map/ppermute | solution.py:23
  249.0 19.9 %collective-permute-start.4 = (bf16[4,1,48,2048]{3,2,1,0:T(8,128)(2,1)S(1)}, bf16[4,1,48,2048]{3,2,1,0:T(8,128)(2,1)S(1)}, u32[]{:S(2)}, u32[]{:S(2)}) collective-permute-start(bf16[4,1,48,2048]{3,2,1,0:T(8,128)(2,1)S(1)} %collective-permute-done.2), channel_id=1, source_target_pairs={{0,1},{1,2},{2,3},{3,4},{4,5},{5,6},{6,7},{7,0},{8,9},{9,10},{10,1... | collective-permute-start | bytes 2359304 | tf_op jit(solution)/shard_map/ppermute | solution.py:18
  249.0 1.1 copy-start.2
  250.3 20.6 %collective-permute-start.5 = (bf16[4,1,48,2048]{3,2,1,0:T(8,128)(2,1)S(1)}, bf16[4,1,48,2048]{3,2,1,0:T(8,128)(2,1)S(1)}, u32[]{:S(2)}, u32[]{:S(2)}) collective-permute-start(bf16[4,1,48,2048]{3,2,1,0:T(8,128)(2,1)S(1)} %collective-permute-done.3), channel_id=1, source_target_pairs={{0,7},{1,0},{2,1},{3,2},{4,3},{5,4},{6,5},{7,6},{8,15},{9,8},{10,9... | collective-permute-start | bytes 2359304 | tf_op jit(solution)/shard_map/ppermute | solution.py:23
  269.0 13.2 %collective-permute-start.6 = (bf16[4,1,48,2048]{3,2,1,0:T(8,128)(2,1)S(1)}, bf16[4,1,48,2048]{3,2,1,0:T(8,128)(2,1)S(1)}, u32[]{:S(2)}, u32[]{:S(2)}) collective-permute-start(bf16[4,1,48,2048]{3,2,1,0:T(8,128)(2,1)S(1)} %collective-permute-done.4), channel_id=1, source_target_pairs={{0,1},{1,2},{2,3},{3,4},{4,5},{5,6},{6,7},{7,0},{8,9},{9,10},{10,1... | collective-permute-start | bytes 2359304 | tf_op jit(solution)/shard_map/ppermute | solution.py:18
  269.1 13.2 %copy-start.8 = (bf16[1,2048,896]{2,1,0:T(8,128)(2,1)S(1)}, bf16[1,2048,896]{2,1,0:T(8,128)(2,1)}, u32[]{:S(2)}) copy-start(bf16[1,2048,896]{2,1,0:T(8,128)(2,1)} %param.25) | copy-start | bytes 11010052
  282.3 6.8 %copy-start.9 = (bf16[1,2048,896]{2,1,0:T(8,128)(2,1)S(1)}, bf16[1,2048,896]{2,1,0:T(8,128)(2,1)}, u32[]{:S(2)}) copy-start(bf16[1,2048,896]{2,1,0:T(8,128)(2,1)} %param.26) | copy-start | bytes 11010052
  289.0 7.3 %copy-start.10 = (bf16[1,896,2048]{2,1,0:T(8,128)(2,1)S(1)}, bf16[1,896,2048]{2,1,0:T(8,128)(2,1)}, u32[]{:S(2)}) copy-start(bf16[1,896,2048]{2,1,0:T(8,128)(2,1)} %param.27) | copy-start | bytes 11010052
  305.0 70.6 %copy-start.7 = (f32[48,2]{0,1:T(2,128)S(1)}, f32[48,2]{0,1:T(2,128)}, u32[]{:S(2)}) copy-start(f32[48,2]{0,1:T(2,128)} %param.29) | copy-start | bytes 1156
  371.6 12.7 %all-to-all-start.2 = ((bf16[4,1,48,2048]{3,2,1,0:T(8,128)(2,1)}), bf16[4,1,48,2048]{3,2,1,0:T(8,128)(2,1)S(1)}, u32[]{:S(2)}, u32[]{:S(2)}) async-start(bf16[4,1,48,2048]{3,2,1,0:T(8,128)(2,1)} %bitcast.100), calls=%async_computation.3 | async-start | bytes 1572864 | tf_op jit(solution)/shard_map/all_to_all | solution.py:179
Sparse Core Ops, SparseCore 0:
  8.9 84.7 all-gather.1
  305.2 66.4 reduce-scatter.1
